TPU v7x, 32 devices: a whole 2x2x4 slice. The times are simulated.
32 devices in a mesh: sp: 8 (over z, y), tp: 4 (over x, core).
Axes of the slice: x: 2, y: 2, z: 4, core: 2. Of those that a mesh axis runs over, the one named last changes fastest.
Arguments:
- tokens: bfloat16 [3072, 2048], P('sp', 'tp'), may hold values from -16 to 16
- norm_gain: bfloat16 [2048], replicated, may hold values from 0.099609375 to 1.8984375
- w_query: bfloat16 [2048, 1024], P(None, 'tp'), may hold values from -0.125 to 0.125
- w_key: bfloat16 [2048, 1024], P(None, 'tp'), may hold values from -0.125 to 0.125
- w_value: bfloat16 [2048, 1024], P(None, 'tp'), may hold values from -0.125 to 0.125
- key_bias: bfloat16 [8, 3072], P('tp', 'sp'), may hold values from -13 to 0
- w_glu_value: bfloat16 [2048, 1024], P(None, 'tp'), may hold values from -0.125 to 0.125
- w_glu_gate: bfloat16 [2048, 1024], P(None, 'tp'), may hold values from -0.125 to 0.125
- conv_weight: bfloat16 [31, 1024], replicated, may hold values from -4 to 4
- conv_bias: bfloat16 [1024], replicated, may hold values from 0 to 16
- ln_gain: bfloat16 [1024], replicated, may hold values from 0.099609375 to 1.8984375
- w_out_att: bfloat16 [1024, 2048], replicated, may hold values from -0.75 to 0.75
- w_out_conv: bfloat16 [1024, 2048], replicated, may hold values from -0.1875 to 0.1875
Outputs:
- mixed: bfloat16 [3072, 2048], P(('sp', 'tp'))
- weight_log: float32 [8, 3072], P('tp', 'sp')
All inputs are finite; a program needn't handle non-finite values.
Results may differ from a plain program's by a relative error of at most 0.007.
Values may be sent and summed in bfloat16 or wider, within the bound.
A program may use at most 192 MiB of HBM per device.

v0:
```python
import jax
import jax.numpy as jnp
from jax import lax
from jax.sharding import PartitionSpec as P

D = 2048
HEAD = 128
CF_WIDTH = 1024


epsilon = 1e-06


def from_behind(block, axis, distance):
    devices = range(lax.axis_size(axis))
    route = [(i - distance, i) for i in devices if i - distance in devices]
    return lax.ppermute(block, axis, route)


def rounded(values):
    return lax.optimization_barrier(values.astype(jnp.bfloat16)).astype(jnp.float32)


def later_matrix(count):
    row_ids = lax.broadcasted_iota(jnp.int32, (count, count), 0)
    col_ids = lax.broadcasted_iota(jnp.int32, (count, count), 1)
    return (row_ids > col_ids).astype(jnp.float32)


def block_terms(query_matrix_rows, key_rows, value_rows, bias_rows):
    head_size = query_matrix_rows.shape[-1]
    scores = jnp.einsum(
        "qhe,khe->hqk", query_matrix_rows, key_rows, preferred_element_type=jnp.float32
    )
    scores = scores * head_size ** (-0.5) + bias_rows.astype(jnp.float32)[:, None, :]
    keep_log = jax.nn.log_sigmoid(-scores)
    row_ids = lax.broadcasted_iota(jnp.int32, scores.shape, 1)
    col_ids = lax.broadcasted_iota(jnp.int32, scores.shape, 2)
    allowed = col_ids <= row_ids
    keep_log = jnp.where(allowed, keep_log, 0.0)
    later_sum = jnp.einsum(
        "hqj,jk->hqk", keep_log, later_matrix(scores.shape[2]), precision=lax.Precision.HIGHEST
    )
    weights = jnp.exp(jax.nn.log_sigmoid(scores) + later_sum)
    weights = jnp.where(allowed, weights, 0.0)
    block_out = jnp.einsum(
        "hqk,khe->qhe", weights.astype(jnp.bfloat16), value_rows, preferred_element_type=jnp.float32
    )
    return (block_out, jnp.sum(keep_log, axis=2))


def window_terms(query_matrix_rows, key_window, value_window, bias_window, valid_count):
    tok_rows, heads_here, head_size = query_matrix_rows.shape
    block_count = key_window.shape[0] // tok_rows
    key_blocks = key_window.reshape(block_count, tok_rows, heads_here, head_size)
    value_blocks = value_window.reshape(block_count, tok_rows, heads_here, head_size)
    bias_blocks = bias_window.astype(jnp.float32).reshape(heads_here, block_count, tok_rows)
    scores = jnp.einsum(
        "qhe,bkhe->hqbk", query_matrix_rows, key_blocks, preferred_element_type=jnp.float32
    )
    scores = scores * head_size ** (-0.5) + bias_blocks[:, None, :, :]
    block_ids = lax.broadcasted_iota(jnp.int32, scores.shape, 2)
    valid = block_ids < valid_count
    keep_log = jnp.where(valid, jax.nn.log_sigmoid(-scores), 0.0)
    later_sum = jnp.einsum(
        "hqbj,jk->hqbk", keep_log, later_matrix(tok_rows), precision=lax.Precision.HIGHEST
    )
    weights = jnp.where(valid, jnp.exp(jax.nn.log_sigmoid(scores) + later_sum), 0.0)
    block_out = jnp.einsum(
        "hqbk,bkhe->bqhe",
        weights.astype(jnp.bfloat16),
        value_blocks,
        preferred_element_type=jnp.float32,
    )
    totals = jnp.sum(keep_log, axis=3)
    after = jnp.einsum(
        "hqj,jb->hqb", totals, later_matrix(block_count), precision=lax.Precision.HIGHEST
    )
    factor = jnp.transpose(jnp.exp(after), (2, 1, 0))[:, :, :, None]
    return (jnp.sum(factor * block_out, axis=0), jnp.sum(totals, axis=2))


def combine(attended_sum, carried, block_out, block_keep):
    factor = jnp.exp(carried).T[:, :, None]
    return (attended_sum + factor * block_out, carried + block_keep)


def on_device(
    tokens,
    norm_gain,
    w_query,
    w_key,
    w_value,
    key_bias,
    w_glu_value,
    w_glu_gate,
    conv_weight,
    conv_bias,
    ln_gain,
    w_out_att,
    w_out_conv,
):
    tok_rows = tokens.shape[0]
    tp_count = lax.axis_size("tp")
    tp_index = lax.axis_index("tp")
    sp_index = lax.axis_index("sp")
    squares = jnp.sum(jnp.square(tokens.astype(jnp.float32)), axis=1)
    row_scale = lax.rsqrt(lax.psum(squares, "tp") / D + epsilon)
    matrices = (w_query, w_key, w_value, w_glu_value, w_glu_gate)
    gain_piece = norm_gain.astype(jnp.float32)
    normed = (
        lax.all_gather(tokens, "tp", axis=1, tiled=True).astype(jnp.float32)
        * row_scale[:, None]
        * gain_piece
    ).astype(jnp.bfloat16)
    projected = tuple(
        (jnp.dot(normed, matrix, preferred_element_type=jnp.float32) for matrix in matrices)
    )
    heads_here = w_query.shape[1] // HEAD
    query_matrix_rows = projected[0].astype(jnp.bfloat16).reshape(tok_rows, heads_here, HEAD)
    key_rows = projected[1].astype(jnp.bfloat16).reshape(tok_rows, heads_here, HEAD)
    value_rows = projected[2].astype(jnp.bfloat16).reshape(tok_rows, heads_here, HEAD)
    glu_value = rounded(projected[3])
    glu_gate = rounded(projected[4])
    attended_sum, carried = block_terms(query_matrix_rows, key_rows, value_rows, key_bias)
    every_key, every_value, every_bias = (
        lax.all_gather(key_rows, "sp", axis=0, tiled=True),
        lax.all_gather(value_rows, "sp", axis=0, tiled=True),
        lax.all_gather(key_bias, "sp", axis=1, tiled=True),
    )
    window_out, window_keep = window_terms(
        query_matrix_rows, every_key, every_value, every_bias, sp_index
    )
    attended_sum, carried = combine(attended_sum, carried, window_out, window_keep)
    attended = attended_sum.astype(jnp.bfloat16).reshape(tok_rows, heads_here * HEAD)
    weight_log = jnp.log(-jnp.expm1(carried))
    channels_here = w_glu_value.shape[1]
    channel_start = tp_index * channels_here
    taps_here = lax.dynamic_slice_in_dim(conv_weight, channel_start, channels_here, 1)
    bias_here = lax.dynamic_slice_in_dim(conv_bias, channel_start, channels_here, 0).astype(
        jnp.float32
    )
    gain_here = lax.dynamic_slice_in_dim(ln_gain, channel_start, channels_here, 0).astype(
        jnp.float32
    )
    gated = (glu_value * jax.nn.sigmoid(glu_gate)).astype(jnp.bfloat16)
    rim_width = conv_weight.shape[0] - 1
    rim_rows = from_behind(gated[tok_rows - rim_width :], "sp", 1)
    extended = jnp.concatenate([rim_rows, gated], axis=0)
    convolved = lax.conv_general_dilated(
        extended[None],
        taps_here[:, None, :],
        (1,),
        [(0, 0)],
        dimension_numbers=("NWC", "WIO", "NWC"),
        feature_group_count=channels_here,
        preferred_element_type=jnp.float32,
    )[0]
    convolved = convolved + bias_here[None, :]
    channel_mean = lax.psum(jnp.sum(convolved, axis=1), "tp") / CF_WIDTH
    centered = convolved - channel_mean[:, None]
    channel_var = lax.psum(jnp.sum(centered * centered, axis=1), "tp") / CF_WIDTH
    conv_out = jax.nn.silu(centered * lax.rsqrt(channel_var + epsilon)[:, None] * gain_here).astype(
        jnp.bfloat16
    )
    att_width = attended.shape[1]
    att_weight = lax.dynamic_slice_in_dim(w_out_att, tp_index * att_width, att_width, 0)
    conv_rows_weight = lax.dynamic_slice_in_dim(w_out_conv, channel_start, channels_here, 0)
    first = jnp.dot(attended, att_weight, preferred_element_type=jnp.float32)
    second = jnp.dot(
        lax.slice_in_dim(conv_out, 0, tok_rows // tp_count * lax.axis_size("tp"), axis=0),
        conv_rows_weight,
        preferred_element_type=jnp.float32,
    )
    mixed = lax.psum_scatter(first + second, "tp", scatter_dimension=0, tiled=True).astype(
        jnp.bfloat16
    )
    return (mixed, weight_log)


def solution(mesh):
    in_specs = (
        P("sp", "tp"),
        P(),
        P(None, "tp"),
        P(None, "tp"),
        P(None, "tp"),
        P("tp", "sp"),
        P(None, "tp"),
        P(None, "tp"),
        P(),
        P(),
        P(),
        P(),
        P(),
    )
    out_specs = (P(("sp", "tp"), None), P("tp", "sp"))
    return jax.shard_map(
        on_device, mesh=mesh, in_specs=in_specs, out_specs=out_specs, check_vma=False
    )
```

profile of v0, /device:TPU:29, one launch (start us, length us, event | category | flops | bytes accessed | tf_op | source)
XLA Modules:
  0.0 179.5 jit_solution(2660870203256576240)
XLA Ops:
  7.2 0.7 all-gather.4.cloned.1.call-update
  8.0 0.7 convert_element_type.66
  8.7 1.2 multiply_reduce_fusion
  9.8 5.7 %psum.21 = f32[384]{0:T(512)S(1)} all-reduce(f32[384]{0:T(512)S(1)} %multiply_reduce_fusion), channel_id=1, replica_groups=mesh['sp'=8,'tp'=4] {'tp'}, use_global_device_ids=true, to_apply=%region_1.0 | all-reduce | flops 384 | bytes 3072 | tf_op jit(solution)/shard_map/psum | solution.py:108
  15.5 15.0 %all-gather.4.cloned.1.call-done = bf16[384,2048]{1,0:T(8,128)(2,1)} async-done(((bf16[384,512]{1,0:T(8,128)(2,1)}), bf16[384,2048]{1,0:T(8,128)(2,1)}) %all-gather.4.cloned.1.call-update) | async-done | bytes 1572880 | tf_op jit(solution)/shard_map/all_gather | solution.py:112
  30.5 3.1 %convolution_convert_fusion.2 = bf16[384,256]{0,1:T(8,128)(2,1)} fusion(bf16[2048,256]{1,0:T(8,128)(2,1)S(1)} %copy-done, bf16[384,2048]{1,0:T(8,128)(2,1)} %all-gather.4.cloned.1.call-done, f32[2048]{0:T(1024)S(1)} %convert_element_type.66, f32[384]{0:T(512)S(1)} %add_rsqrt_fusion.1), kind=kOutput, calls=%fused_computation.35 | convolution fusion | flops 405897216 | bytes 2827776 | tf_op jit(solution)/shard_map/dot_general | solution.py:117
  33.7 21.4 %all_gather.14 = bf16[2,3072]{1,0:T(2,128)(2,1)S(1)} all-gather(bf16[2,384]{1,0:T(2,128)(2,1)S(1)} %copy-done.3), channel_id=1, replica_groups=mesh['sp'=8,'tp'=4] {'sp'}, dimensions={1}, use_global_device_ids=true | all-gather | bytes 13824 | tf_op jit(solution)/shard_map/all_gather | solution.py:129
  55.2 0.8 dynamic-slice_convert_fusion.1
  56.0 0.8 dynamic-slice_convert_fusion
  56.8 0.7 dynamic-slice_bitcast_fusion
  57.5 1.8 %convolution_convert_fusion.1 = bf16[384,256]{1,0:T(8,128)(2,1)S(1)} fusion(bf16[2048,256]{1,0:T(8,128)(2,1)} %param.19, bf16[384,2048]{1,0:T(8,128)(2,1)S(1)} %copy-done.4, f32[2048]{0:T(1024)S(1)} %convert_element_type.66, f32[384]{0:T(512)S(1)} %add_rsqrt_fusion.1), kind=kOutput, calls=%fused_computation.34 | convolution fusion | flops 405897216 | bytes 2827776 | tf_op jit(solution)/shard_map/dot_general | solution.py:117
  59.4 0.6 convolution_convert_fusion
  60.2 1.4 collective-permute-start
  61.6 0.9 convolution_convert_fusion.3
  62.5 0.4 fusion.39
  63.0 0.9 convolution_convert_fusion.4
  63.8 2.7 %fusion.15 = bf16[2,384,384]{1,2,0:T(8,128)(2,1)} fusion(f32[2,384,384]{1,2,0:T(8,128)S(1)} %get-tuple-element.7, u8[384,384]{0,1:T(8,128)(4,1)S(1)} %get-tuple-element.6), kind=kOutput, calls=%fused_computation.24 | convolution fusion | flops 1366179840 | bytes 1916928 | tf_op jit(solution)/shard_map/hqj,jk->hqk/dot_general | solution.py:41
  66.5 0.6 fusion.23
  67.1 0.8 copy.31
  68.2 1.0 convolution_select_fusion
  69.5 8.5 %psum.22 = f32[384]{0:T(512)S(1)} all-reduce(f32[384]{0:T(512)S(1)} %fusion.38), channel_id=1, replica_groups=mesh['sp'=8,'tp'=4] {'tp'}, use_global_device_ids=true, to_apply=%region_6.7 | all-reduce | flops 384 | bytes 3072 | tf_op jit(solution)/shard_map/psum | solution.py:160
  78.3 6.2 %psum.23 = f32[384]{0:T(512)S(1)} all-reduce(f32[384]{0:T(512)S(1)} %multiply_reduce_fusion.1), channel_id=1, replica_groups=mesh['sp'=8,'tp'=4] {'tp'}, use_global_device_ids=true, to_apply=%region_8.9 | all-reduce | flops 384 | bytes 3072 | tf_op jit(solution)/shard_map/psum | solution.py:162
  84.5 1.9 %copy.28 = bf16[3072,2,128]{2,0,1:T(8,128)(2,1)S(1)} copy(bf16[3072,2,128]{0,2,1:T(8,128)(2,1)} %all-gather.6.cloned.1.call-done) | data formatting | bytes 3145728 | tf_op jit(solution)/shard_map/all_gather | solution.py:127
  86.4 3.4 %fusion.8 = (u8[2,384,384]{1,2,0:T(8,128)(4,1)S(1)}, f32[2,384,8,384]{1,3,2,0:T(8,128)S(1)}) fusion(f32[2,8,384]{2,1,0:T(8,128)S(1)} %bitcast.79, bf16[384,2,128,1]{0,2,3,1:T(8,128)(2,1)S(1)} %bitcast.78, bf16[8,384,2,128]{3,1,0,2:T(8,128)(2,1)S(1)} %bitcast.71), kind=kOutput, calls=%fused_computation.17 | convolution fusion | flops 620199936 | bytes 11526144 | tf_op jit(solution)/shard_map/qhe,bkhe->hqbk/dot_general | solution.py:58
  89.8 7.6 %fusion.58 = (f32[2,384]{1,0:T(2,128)S(1)}, f32[2,384,8]{1,2,0:T(8,128)S(1)}) fusion(f32[2,8,384]{2,1,0:T(8,128)S(1)} %bitcast.80, f32[2,384,8,384]{1,3,2,0:T(8,128)S(1)} %get-tuple-element.9, u8[2,384,384]{1,2,0:T(8,128)(4,1)S(1)} %get-tuple-element.8, pred[8]{0:T(512)(128)(4,1)S(1)} %iota_compare_fusion.4), kind=kLoop, calls=%fused_computation.94 | loop fusion | flops 35382528 | bytes 9784328 | tf_op jit(solution)/shard_map/reduce_sum | solution.py:80
  97.6 0.6 negate_log_fusion
  98.2 23.3 %fusion.4 = bf16[2,384,8,384]{1,3,2,0:T(8,128)(2,1)} fusion(f32[2,384,8,384]{1,3,2,0:T(8,128)S(1)} %get-tuple-element.9, f32[2,8,384]{2,1,0:T(8,128)S(1)} %bitcast.81, pred[8]{0:T(512)(128)(4,1)S(1)} %iota_compare_fusion.4, u8[2,384,384]{1,2,0:T(8,128)(4,1)S(1)} %get-tuple-element.8), kind=kOutput, calls=%fused_computation.5 | convolution fusion | flops 10933125120 | bytes 14475272 | tf_op jit(solution)/shard_map/hqbj,jk->hqbk/dot_general | solution.py:65
  121.5 4.1 %fusion.7 = f32[384,2,128]{0,2,1:T(8,128)S(1)} fusion(bf16[2,384,8,384]{1,3,2,0:T(8,128)(2,1)} %fusion.4, bf16[8,384,2,128]{3,1,0,2:T(8,128)(2,1)} %bitcast.83, f32[8,384,2]{1,2,0:T(2,128)S(1)} %copy.30), kind=kOutput, calls=%fused_computation.14 | convolution fusion | flops 605454336 | bytes 6709248 | tf_op jit(solution)/shard_map/hqbk,bkhe->bqhe/dot_general | solution.py:69
  125.9 1.8 %fusion.21 = f32[384,2048]{1,0:T(8,128)S(1)} fusion(bf16[384,256]{0,1:T(8,128)(2,1)S(1)} %bitcast.72, bf16[1024,2048]{1,0:T(8,128)(2,1)} %param.24, s32[]{:T(128)S(6)} %select_n.45), kind=kOutput, calls=%fused_computation.42 | convolution fusion | flops 402653184 | bytes 4390916 | tf_op jit(solution)/shard_map/dot_general | solution.py:169
  127.7 3.6 %convolution_add_fusion = f32[384,2048]{1,0:T(8,128)} fusion(f32[384,2048]{1,0:T(8,128)S(1)} %fusion.21, bf16[1024,2048]{1,0:T(8,128)(2,1)} %param.25, s32[]{:T(128)S(6)} %select_n.45, f32[1,416,256]{2,1,0:T(8,128)S(1)} %reshape.44, f32[256]{0:T(256)S(1)} %dynamic-slice_convert_fusion, f32[384]{0:T(512)S(1)} %add_rsqrt_fusion, ...), kind=kOutput, calls=%fused_computation.16 | convolution fusion | flops 404324352 | bytes 7739396 | tf_op jit(solution)/shard_map/dot_general | solution.py:170
  131.4 39.7 %reduce-scatter.2.cloned.1.call-done = f32[96,2048]{1,0:T(8,128)} async-done(((f32[384,2048]{1,0:T(8,128)}), f32[96,2048]{1,0:T(8,128)}) %reduce-scatter.2.cloned.1.call-update) | async-done | bytes 786448 | tf_op jit(solution)/shard_map/reduce_scatter | solution.py:175
  171.0 1.9 %convert_element_type.83 = bf16[96,2048]{1,0:T(8,128)(2,1)} convert(f32[96,2048]{1,0:T(8,128)} %reduce-scatter.2.cloned.1.call-done) | non-fusion elementwise | flops 196608 | bytes 1179648 | tf_op jit(solution)/shard_map/convert_element_type | solution.py:175
  (48 shorter events, 1.6 us)
Async XLA Ops:
  7.2 23.4 %copy-start = (bf16[2048,256]{1,0:T(8,128)(2,1)S(1)}, bf16[2048,256]{1,0:T(8,128)(2,1)}, u32[]{:S(2)}) copy-start(bf16[2048,256]{1,0:T(8,128)(2,1)} %param.16) | copy-start | bytes 3145732
  7.2 26.5 %copy-start.3 = (bf16[2,384]{1,0:T(2,128)(2,1)S(1)}, bf16[2,384]{1,0:T(2,128)(2,1)}, u32[]{:S(2)}) copy-start(bf16[2,384]{1,0:T(2,128)(2,1)} %param.18) | copy-start | bytes 4612
  7.2 23.4 %all-gather.4.cloned.1.call-start = ((), (), s32[]{:S(2)}) async-start(), calls=%async_computation.1 | async-start | bytes 1966080 | tf_op jit(solution)/shard_map/all_gather | solution.py:112
  7.9 76.5 %all-gather.6.cloned.1.call-start = ((), (), s32[]{:S(2)}) async-start(), calls=%async_computation.2 | async-start | bytes 1769472 | tf_op jit(solution)/shard_map/all_gather | solution.py:127
  30.5 26.9 %copy-start.4 = (bf16[384,2048]{1,0:T(8,128)(2,1)S(1)}, bf16[384,2048]{1,0:T(8,128)(2,1)}, u32[]{:S(2)}) copy-start(bf16[384,2048]{1,0:T(8,128)(2,1)} %all-gather.4.cloned.1.call-done) | copy-start | bytes 4718596
  33.6 87.8 %all-gather.8.cloned.1.call-start = ((), (), s32[]{:S(2)}) async-start(), calls=%async_computation.3 | async-start | bytes 1769472 | tf_op jit(solution)/shard_map/all_gather | solution.py:128
  55.2 4.2 %copy-start.5 = (bf16[2048,256]{1,0:T(8,128)(2,1)S(1)}, bf16[2048,256]{1,0:T(8,128)(2,1)}, u32[]{:S(2)}) copy-start(bf16[2048,256]{1,0:T(8,128)(2,1)} %param.20) | copy-start | bytes 3145732
  59.4 2.2 %copy-start.6 = (bf16[2048,256]{1,0:T(8,128)(2,1)S(1)}, bf16[2048,256]{1,0:T(8,128)(2,1)}, u32[]{:S(2)}) copy-start(bf16[2048,256]{1,0:T(8,128)(2,1)} %param.15) | copy-start | bytes 3145732
  60.0 2.5 %copy-start.1 = (bf16[384,256]{0,1:T(8,128)(2,1)S(1)}, bf16[384,256]{0,1:T(8,128)(2,1)}, u32[]{:S(2)}) copy-start(bf16[384,256]{0,1:T(8,128)(2,1)} %convolution_convert_fusion.2) | copy-start | bytes 589828
  60.0 2.9 %copy-start.7 = (bf16[2048,256]{1,0:T(8,128)(2,1)S(1)}, bf16[2048,256]{1,0:T(8,128)(2,1)}, u32[]{:S(2)}) copy-start(bf16[2048,256]{1,0:T(8,128)(2,1)} %param.17) | copy-start | bytes 3145732
  60.2 7.8 %collective-permute-start = (bf16[30,256]{1,0:T(8,128)(2,1)S(1)}, bf16[30,256]{1,0:T(8,128)(2,1)S(1)}, u32[]{:S(2)}, u32[]{:S(2)}) collective-permute-start(bf16[30,256]{1,0:T(8,128)(2,1)S(1)} %slice.6), channel_id=1, source_target_pairs={{0,4},{4,8},{8,12},{12,16},{16,20},{20,24},{24,28},{1,5},{5,9},{9,... | collective-permute-start | bytes 46088 | tf_op jit(solution)/shard_map/ppermute | solution.py:17
  66.5 1.7 copy-start.8
  67.9 103.1 %reduce-scatter.2.cloned.1.call-start = ((), (), s32[]{:S(2)}) async-start(), calls=%async_computation.4 | async-start | bytes 3932160 | tf_op jit(solution)/shard_map/reduce_scatter | solution.py:175
  121.5 4.2 %copy-start.2 = (bf16[2,384,384]{1,2,0:T(8,128)(2,1)S(1)}, bf16[2,384,384]{1,2,0:T(8,128)(2,1)}, u32[]{:S(2)}) copy-start(bf16[2,384,384]{1,2,0:T(8,128)(2,1)} %fusion.15) | copy-start | bytes 1769476
Sparse Core Ops, SparseCore 0:
  9.6 20.9 all-gather.3
  33.8 39.9 all-gather.5
  75.9 43.8 all-gather.7
  131.5 39.4 reduce-scatter.1
where the time goes:
time: 182 us; the launch traced here: 179 us
  waiting for transfers between devices  55.4 us (30%)
  matrix products  48 us (26%)
  blocking collectives  41.8 us (23%)
  other arithmetic  14.7 us (8%)
  between operations  14.1 us (8%)
  local copies, waits for them, and re-layouts  3.85 us (2%)
    reduce_scatter x1, waiting for transfers between devices, on_device(): lax.psum_scatter(first + second, 'tp', scatter_dimension=0, tiled=True)  39.7 us
    dot_general x1, matrix products, window_terms(): jnp.einsum('hqbj,jk->hqbk', keep_log, later_matrix(tok_rows), precision=l...  23.3 us
    all_gather x1, blocking collectives, on_device(): lax.all_gather(key_bias, 'sp', axis=1, tiled=True)  21.4 us
    all_gather x1, waiting for transfers between devices, on_device(): lax.all_gather(tokens, 'tp', axis=1, tiled=True).astype(jnp.float32)  15 us
    psum x1, blocking collectives, on_device(): channel_mean = lax.psum(jnp.sum(convolved, axis=1), 'tp') / CF_WIDTH  8.51 us
    reduce_sum x1, other arithmetic, window_terms(): return (jnp.sum(factor * block_out, axis=0), jnp.sum(totals, axis=2))  7.62 us
    dot_general x5, matrix products, on_device(): jnp.dot(normed, matrix, preferred_element_type=jnp.float32)  7.29 us
    psum x1, blocking collectives, on_device(): lax.psum(jnp.sum(centered * centered, axis=1), 'tp') / CF_WIDTH  6.16 us
  transfers between devices with their start and end apart: 5, of which 2 were waited for; matrix products, arithmetic and copies ran while one was open for 29% of the time, Pallas kernels for 0%

commit v1 on v0

v1 whole, which is shorter than its diff:
```python
import functools

import jax
import jax.numpy as jnp
from jax import lax
from jax.experimental import pallas as pl
from jax.experimental.pallas import tpu as pltpu
from jax.sharding import PartitionSpec as P

HEAD = 128

epsilon = 1e-06
MESH = pl.DeviceIdType.MESH
VMEM_LIMIT = 56 * 1024 * 1024


def from_behind(block, axis, distance):
    devices = range(lax.axis_size(axis))
    route = [(i - distance, i) for i in devices if i - distance in devices]
    return lax.ppermute(block, axis, route)


def flip(index, bit):
    return index + bit - 2 * bit * ((index // bit) % 2)


def greet(peers, axis):
    barrier = pltpu.get_barrier_semaphore()
    for peer in peers:
        pl.semaphore_signal(barrier, inc=1, device_id={axis: peer}, device_id_type=MESH)
    pl.semaphore_wait(barrier, len(peers))


def project_kernel(
    n, chunks, tok, gain, wq, wk, wv, wgv, wgg, q, k, v, gated, slots, normed, send, recv
):
    me = lax.axis_index("tp")
    rows, width = tok.shape
    step = rows // chunks
    bits = []
    bit = n // 2
    while bit >= 1:
        bits.append(bit)
        bit //= 2
    greet([flip(me, bit) for bit in bits], "tp")

    routes, held = [], [()]
    for bit in bits:
        routes.append(list(held))
        held = held + [path + (bit,) for path in held]

    def owner_of(path):
        owner = me
        for bit in path:
            owner = flip(owner, bit)
        return owner

    index = {}
    for stage, bit in enumerate(bits):
        for path in routes[stage]:
            index[(stage, path)] = len(index)

    def copy_of(stage, path, chunk):
        part = pl.ds(chunk * step, step)
        owner = owner_of(path)
        source = tok.at[part] if path == () else slots.at[owner, part]
        at = index[(stage, path)]
        return pltpu.make_async_remote_copy(
            src_ref=source,
            dst_ref=slots.at[owner, part],
            send_sem=send.at[at, chunk],
            recv_sem=recv.at[at, chunk],
            device_id={"tp": flip(me, bits[stage])},
            device_id_type=MESH,
        )

    for chunk in range(chunks):
        for stage in range(len(bits)):
            copy_of(stage, (), chunk).start()

    def forward(chunk):
        for stage in range(len(bits) - 1):
            for path in routes[stage]:
                copy_of(stage, path, chunk).wait_recv()
                new = path + (bits[stage],)
                for later in range(stage + 1, len(bits)):
                    copy_of(later, new, chunk).start()

    def work(chunk):
        last = len(bits) - 1
        for path in routes[last]:
            copy_of(last, path, chunk).wait_recv()
        part = pl.ds(chunk * step, step)
        squares = jnp.zeros((step, 1), jnp.float32)
        for path in held:
            x = tok[part, :] if path == () else slots[owner_of(path), part, :]
            x = x.astype(jnp.float32)
            squares = squares + jnp.sum(x * x, axis=1, keepdims=True)
        scale = lax.rsqrt(squares / (width * n) + epsilon)
        for path in held:
            owner = owner_of(path)
            x = tok[part, :] if path == () else slots[owner, part, :]
            y = x.astype(jnp.float32) * scale * gain[owner].astype(jnp.float32)
            normed[:, pl.ds(pl.multiple_of(owner * width, width), width)] = y.astype(jnp.bfloat16)

        def project(matrix):
            return jnp.dot(normed[...], matrix[...], preferred_element_type=jnp.float32).astype(
                jnp.bfloat16
            )

        q[part, :] = project(wq)
        k[part, :] = project(wk)
        v[part, :] = project(wv)
        value = project(wgv).astype(jnp.float32)
        gate = project(wgg).astype(jnp.float32)
        gated[part, :] = (value * jax.nn.sigmoid(gate)).astype(jnp.bfloat16)

    for chunk in range(chunks):
        forward(chunk)
        if chunk > 0:
            work(chunk - 1)
    work(chunks - 1)
    for chunk in range(chunks):
        for stage in range(len(bits)):
            for path in routes[stage]:
                copy_of(stage, path, chunk).wait_send()


def attention_tile(q, k, v, bias, later, row_start, masked):
    scores = lax.dot_general(q, k, (((1,), (1,)), ((), ())), preferred_element_type=jnp.float32)
    scores = scores * q.shape[1] ** (-0.5) + bias
    small = jnp.exp(-jnp.abs(scores))
    soft = jnp.where(
        small < 4e-3, small * (1.0 - small * (0.5 - small * (1.0 / 3.0))), jnp.log(1.0 + small)
    )
    keep = jnp.minimum(-scores, 0.0) - soft
    log_weight = jnp.minimum(scores, 0.0) - soft
    if masked:
        row_ids = lax.broadcasted_iota(jnp.int32, scores.shape, 0) + row_start
        col_ids = lax.broadcasted_iota(jnp.int32, scores.shape, 1)
        allowed = col_ids <= row_ids
        keep = jnp.where(allowed, keep, 0.0)
    high = keep.astype(jnp.bfloat16)
    low = (keep - high.astype(jnp.float32)).astype(jnp.bfloat16)
    after = jnp.dot(high, later, preferred_element_type=jnp.float32) + jnp.dot(
        low, later, preferred_element_type=jnp.float32
    )
    weights = jnp.exp(log_weight + after)
    if masked:
        weights = jnp.where(allowed, weights, 0.0)
    out = jnp.dot(weights.astype(jnp.bfloat16), v, preferred_element_type=jnp.float32)
    return out, jnp.sum(keep, axis=1, keepdims=True)


def fill_later(later):
    row_ids = lax.broadcasted_iota(jnp.int32, later.shape, 0)
    col_ids = lax.broadcasted_iota(jnp.int32, later.shape, 1)
    later[...] = (row_ids > col_ids).astype(jnp.float32).astype(jnp.bfloat16)


def attention_kernel(tile, q, k, v, bias, att, carried_out, later, total, carried):
    me = lax.axis_index("sp")
    rows, width = q.shape
    heads = width // HEAD
    fill_later(later)

    def block_step(block, masked):
        begin = pl.multiple_of(block * rows, rows)
        for head in range(heads):
            cols = pl.ds(head * HEAD, HEAD)
            keys = k[pl.ds(begin, rows), cols]
            values = v[pl.ds(begin, rows), cols]
            offsets = bias[block, pl.ds(head, 1), :].astype(jnp.float32)
            for start in range(0, rows, tile):
                part = pl.ds(start, tile)
                out, kept = attention_tile(
                    q[part, cols], keys, values, offsets, later[...], start, masked
                )
                if masked:
                    total[part, cols] = out
                    carried[head, part, :] = kept
                else:
                    before = carried[head, part, :]
                    total[part, cols] = total[part, cols] + jnp.exp(before) * out
                    carried[head, part, :] = before + kept

    block_step(me, True)

    def absorb(turn, state):
        block_step(me - 1 - turn, False)
        return state

    lax.fori_loop(0, me, absorb, 0)
    att[...] = total[...].astype(jnp.bfloat16)
    lanes = lax.broadcasted_iota(jnp.int32, carried_out.shape, 1)
    result = jnp.zeros(carried_out.shape, jnp.float32)
    for head in range(heads):
        result = jnp.where(lanes == head, carried[head], result)
    carried_out[...] = result


def mix_kernel(n, tile, att, conv, gain, wa, wc, out, att_slots, conv_slots, both, send, recv):
    me = lax.axis_index("tp")
    rows, width = att.shape
    channels = conv.shape[1]
    mine = rows // n
    peers = [lax.rem(me + off, n) for off in range(1, n)]
    greet(peers, "tp")

    def copy_of(off, i):
        peer = lax.rem(me + off, n)
        part = pl.ds(pl.multiple_of(peer * mine, mine), mine)
        source, slots = ((conv, conv_slots), (att, att_slots))[i]
        return pltpu.make_async_remote_copy(
            src_ref=source.at[part],
            dst_ref=slots.at[off - 1],
            send_sem=send.at[i, off - 1],
            recv_sem=recv.at[i, off - 1],
            device_id={"tp": peer},
            device_id_type=MESH,
        )

    for i in range(2):
        for off in range(1, n):
            copy_of(off, i).start()
    own = pl.ds(pl.multiple_of(me * mine, mine), mine)
    for off in range(1, n):
        copy_of(off, 0).wait_recv()
    owners = [me] + [lax.rem(me + n - off, n) for off in range(1, n)]
    pieces = [conv[own, :]] + [conv_slots[off - 1] for off in range(1, n)]
    count = n * channels
    mean = sum(jnp.sum(x, axis=1, keepdims=True) for x in pieces) / count
    centered = [x - mean for x in pieces]
    variance = sum(jnp.sum(x * x, axis=1, keepdims=True) for x in centered) / count
    scale = lax.rsqrt(variance + epsilon)
    for owner, x in zip(owners, centered):
        y = x * scale * gain[owner].astype(jnp.float32)
        y = y * jax.nn.sigmoid(y)
        at = pl.multiple_of(n * width + owner * channels, 128)
        both[:, pl.ds(at, channels)] = y.astype(jnp.bfloat16)
    for off in range(1, n):
        copy_of(off, 1).wait_recv()
    for off, owner in enumerate(owners):
        x = att[own, :] if off == 0 else att_slots[off - 1]
        both[:, pl.ds(pl.multiple_of(owner * width, 128), width)] = x
    for start in range(0, out.shape[1], tile):
        cols = pl.ds(start, tile)
        first = jnp.dot(both[:, : n * width], wa[:, cols], preferred_element_type=jnp.float32)
        second = jnp.dot(both[:, n * width :], wc[:, cols], preferred_element_type=jnp.float32)
        out[:, cols] = (first + second).astype(jnp.bfloat16)
    for off in range(1, n):
        for i in range(2):
            copy_of(off, i).wait_send()


def vmem_specs(count):
    return [pl.BlockSpec(memory_space=pltpu.VMEM)] * count


def largest_tile(rows, limit):
    tile = min(rows, limit)
    while rows % tile:
        tile //= 2
    return tile


def on_device(
    tokens,
    norm_gain,
    w_query,
    w_key,
    w_value,
    key_bias,
    w_glu_value,
    w_glu_gate,
    conv_weight,
    conv_bias,
    ln_gain,
    w_out_att,
    w_out_conv,
):
    tok_rows, feature_width = tokens.shape
    n = lax.axis_size("tp")
    sp_count = lax.axis_size("sp")
    tp_index = lax.axis_index("tp")
    width = w_query.shape[1]
    heads_here = width // HEAD
    channels_here = w_glu_value.shape[1]
    model_width = w_out_att.shape[1]
    bf16, f32 = jnp.bfloat16, jnp.float32
    chunks = tok_rows // largest_tile(tok_rows, 128)
    query, key_rows, value_rows, gated = pl.pallas_call(
        functools.partial(project_kernel, n, chunks),
        out_shape=[jax.ShapeDtypeStruct((tok_rows, width), bf16)] * 3
        + [jax.ShapeDtypeStruct((tok_rows, channels_here), bf16)],
        in_specs=vmem_specs(7),
        out_specs=vmem_specs(4),
        scratch_shapes=[
            pltpu.VMEM((n, tok_rows, feature_width), bf16),
            pltpu.VMEM((tok_rows // chunks, n * feature_width), bf16),
            pltpu.SemaphoreType.DMA((n - 1, chunks)),
            pltpu.SemaphoreType.DMA((n - 1, chunks)),
        ],
        compiler_params=pltpu.CompilerParams(
            collective_id=0, has_side_effects=True, vmem_limit_bytes=VMEM_LIMIT
        ),
        name="project",
    )(
        tokens,
        norm_gain.reshape(n, 1, feature_width),
        w_query,
        w_key,
        w_value,
        w_glu_value,
        w_glu_gate,
    )
    rim_width = conv_weight.shape[0] - 1
    rim_rows = from_behind(gated[tok_rows - rim_width :], "sp", 1)
    every_key = lax.all_gather(key_rows, "sp", axis=0, tiled=True)
    every_value = lax.all_gather(value_rows, "sp", axis=0, tiled=True)
    every_bias = lax.all_gather(key_bias, "sp", axis=0, tiled=False)
    channel_start = tp_index * channels_here
    taps_here = lax.dynamic_slice_in_dim(conv_weight, channel_start, channels_here, 1)
    bias_here = lax.dynamic_slice_in_dim(conv_bias, channel_start, channels_here, 0).astype(f32)
    extended = jnp.concatenate([rim_rows, gated], axis=0)
    convolved = lax.conv_general_dilated(
        extended[None],
        taps_here[:, None, :],
        (1,),
        [(0, 0)],
        dimension_numbers=("NWC", "WIO", "NWC"),
        feature_group_count=channels_here,
        preferred_element_type=f32,
    )[0]
    convolved = convolved + bias_here[None, :]
    tile = largest_tile(tok_rows, 128)
    attended, carried = pl.pallas_call(
        functools.partial(attention_kernel, tile),
        out_shape=[
            jax.ShapeDtypeStruct((tok_rows, width), bf16),
            jax.ShapeDtypeStruct((tok_rows, 128), f32),
        ],
        in_specs=vmem_specs(4),
        out_specs=vmem_specs(2),
        scratch_shapes=[
            pltpu.VMEM((tok_rows, tok_rows), bf16),
            pltpu.VMEM((tok_rows, width), f32),
            pltpu.VMEM((heads_here, tok_rows, 1), f32),
        ],
        compiler_params=pltpu.CompilerParams(vmem_limit_bytes=VMEM_LIMIT),
        name="attention",
    )(query, every_key, every_value, every_bias)
    weight_log = jnp.log(-jnp.expm1(carried[:, :heads_here].T))
    mine = tok_rows // n
    mixed = pl.pallas_call(
        functools.partial(mix_kernel, n, largest_tile(model_width, 512)),
        out_shape=jax.ShapeDtypeStruct((mine, model_width), bf16),
        in_specs=vmem_specs(5),
        out_specs=pl.BlockSpec(memory_space=pltpu.VMEM),
        scratch_shapes=[
            pltpu.VMEM((n - 1, mine, width), bf16),
            pltpu.VMEM((n - 1, mine, channels_here), f32),
            pltpu.VMEM((mine, n * (width + channels_here)), bf16),
            pltpu.SemaphoreType.DMA((2, n - 1)),
            pltpu.SemaphoreType.DMA((2, n - 1)),
        ],
        compiler_params=pltpu.CompilerParams(
            collective_id=1, has_side_effects=True, vmem_limit_bytes=VMEM_LIMIT
        ),
        name="mix",
    )(attended, convolved, ln_gain.reshape(n, 1, channels_here), w_out_att, w_out_conv)
    return (mixed, weight_log)


def solution(mesh):
    in_specs = (
        P("sp", "tp"),
        P(),
        P(None, "tp"),
        P(None, "tp"),
        P(None, "tp"),
        P("tp", "sp"),
        P(None, "tp"),
        P(None, "tp"),
        P(),
        P(),
        P(),
        P(),
        P(),
    )
    out_specs = (P(("sp", "tp"), None), P("tp", "sp"))
    return jax.shard_map(
        on_device, mesh=mesh, in_specs=in_specs, out_specs=out_specs, check_vma=False
    )
```

time: 182 us -> 166 us (0.912); the launches traced: 179 us -> 166 us
  Pallas kernels: 0 us -> 61.4 us
  matrix products: 48 us -> 5.62 us
  blocking collectives: 41.8 us -> 21 us
  other arithmetic: 14.7 us -> 2.61 us
    pallas_call x0 -> x3, Pallas kernels: none -> 61.4 us  [the longest x1 27.9 us: on_device(): pl.pallas_call(functools.partial(attention_kernel, tile), out_shape=[jax....]
    dot_general x14 -> x0, matrix products: 47.1 us -> none  [the longest x1 23.3 us: window_terms(): jnp.einsum('hqbj,jk->hqbk', keep_log, later_matrix(tok_rows), precision=l...]
    reduce_scatter x1 -> x0, waiting for transfers between devices: 39.7 us -> none  [on_device(): lax.psum_scatter(first + second, 'tp', scatter_dimension=0, tiled=True)]
    all_gather x3 -> x2, waiting for transfers between devices: 15 us -> 54 us  [the longest x1 44.7 us: on_device(): every_value = lax.all_gather(value_rows, 'sp', axis=0, tiled=True)]
    psum x3 -> x0, blocking collectives: 20.3 us -> none  [the longest x1 8.51 us: on_device(): channel_mean = lax.psum(jnp.sum(convolved, axis=1), 'tp') / CF_WIDTH]
    reduce_sum x5 -> x0, other arithmetic: 9.71 us -> none  [the longest x1 7.62 us: window_terms(): return (jnp.sum(factor * block_out, axis=0), jnp.sum(totals, axis=2))]
    conv_general_dilated x1, matrix products: 0.97 us -> 5.62 us  [on_device(): lax.conv_general_dilated(extended[None], taps_here[:, None, :], (1,), [(0...]
    convert_element_type x5 -> x0, other arithmetic: 3.49 us -> none  [the longest x1 1.92 us: on_device(): lax.psum_scatter(first + second, 'tp', scatter_dimension=0, tiled=True)]
  transfers between devices with their start and end apart: 5 -> 3, of which waited for: 2 -> 2; matrix products, arithmetic and copies ran while one was open for 29% -> 6% of each run, Pallas kernels for 0% -> 0%
where the time goes in v1:
time: 166 us
  Pallas kernels  61.4 us (37%)
  waiting for transfers between devices  54.7 us (33%)
  blocking collectives  21 us (13%)
  between operations  14.1 us (8%)
  matrix products  5.62 us (3%)
  local copies, waits for them, and re-layouts  5.1 us (3%)
  other arithmetic  2.61 us (2%)
    all_gather x1, waiting for transfers between devices, on_device(): every_value = lax.all_gather(value_rows, 'sp', axis=0, tiled=True)  44.7 us
    pallas_call x1, Pallas kernels, on_device(): pl.pallas_call(functools.partial(attention_kernel, tile), out_shape=[jax....  27.9 us
    all_gather x1, blocking collectives, on_device(): every_bias = lax.all_gather(key_bias, 'sp', axis=0, tiled=False)  21 us
    pallas_call x1, Pallas kernels, on_device(): pl.pallas_call(functools.partial(project_kernel, n, chunks), out_shape=[j...  17.7 us
    pallas_call x1, Pallas kernels, on_device(): pl.pallas_call(functools.partial(mix_kernel, n, largest_tile(model_width,...  15.8 us
    all_gather x1, waiting for transfers between devices, on_device(): every_key = lax.all_gather(key_rows, 'sp', axis=0, tiled=True)  9.22 us
    conv_general_dilated x1, matrix products, on_device(): lax.conv_general_dilated(extended[None], taps_here[:, None, :], (1,), [(0...  5.62 us
  transfers between devices with their start and end apart: 3, of which 2 were waited for; matrix products, arithmetic and copies ran while one was open for 6% of the time, Pallas kernels for 0%

profile of v1, /device:TPU:29, one launch (start us, length us, event | category | flops | bytes accessed | tf_op | source)
XLA Modules:
  0.0 165.8 jit_solution(449263587746815947)
XLA Ops:
  7.2 0.0 copy-start
  7.2 0.0 copy-start.2
  7.2 0.0 copy-start.3
  7.2 0.0 all-gather.5.cloned.1.call-start
  7.2 1.3 reshape.17.gain
  8.5 17.7 %project.1 = (bf16[384,256]{1,0:T(8,128)(2,1)}, bf16[384,256]{1,0:T(8,128)(2,1)}, bf16[384,256]{1,0:T(8,128)(2,1)}, bf16[384,256]{1,0:T(8,128)(2,1)}) custom-call(bf16[384,512]{1,0:T(8,128)(2,1)} %tok.1, bf16[4,1,512]{2,1,0:T(2,128)(2,1)} %reshape.17.gain, bf16[2048,256]{1,0:T(8,128)(2,1)} %wq.1, bf16[2048,256]{1,0:T(8,128)(2,1)} %wk.1, ...), custom_call_target="tpu_custom_call" | custom-call | tf_op jit(solution)/shard_map/project/pallas_call | solution.py:292
  26.3 0.0 all-gather.5.cloned.1.call-update
  26.3 0.0 all-gather.7.cloned.1.call-start
  26.4 0.7 all-gather.7.cloned.1.call-update
  27.1 0.7 slice.6
  27.8 1.3 collective-permute-start
  29.1 0.0 copy-done
  29.1 0.8 dynamic-slice_convert_fusion
  29.9 0.0 copy-done.2
  29.9 0.6 reshape.18.gain
  30.5 0.0 copy-done.3
  30.5 21.0 %all-gather.1.bias = bf16[8,2,384]{2,1,0:T(2,128)(2,1)} all-gather(bf16[1,2,384]{2,1,0:T(2,128)(2,1)S(1)} %bitcast.9), channel_id=2, replica_groups=mesh['sp'=8,'tp'=4] {'sp'}, dimensions={0}, use_global_device_ids=true | all-gather | bytes 13824 | tf_op jit(solution)/shard_map/all_gather | solution.py:321
  51.4 0.0 collective-permute-done
  51.4 1.0 maximum_bitcast_fusion
  52.4 5.6 %fusion = f32[1,384,256]{2,0,1:T(1,128)S(1)} fusion(bf16[1,414,256]{2,1,0:T(8,128)(2,1)S(1)} %maximum_bitcast_fusion, bf16[31,1,256]{2,0,1:T(8,128)(2,1)S(1)} %dynamic-slice_bitcast_fusion), kind=kOutput, calls=%fused_computation | convolution fusion | flops 6094848 | bytes 621056 | tf_op jit(solution)/shard_map/conv_general_dilated | solution.py:326
  58.1 0.8 bitcast_add_fusion.conv
  58.8 9.2 %all-gather.5.cloned.1.call-done.k = bf16[3072,256]{1,0:T(8,128)(2,1)} async-done(((bf16[384,256]{1,0:T(8,128)(2,1)}), bf16[3072,256]{1,0:T(8,128)(2,1)}) %all-gather.5.cloned.1.call-update) | async-done | bytes 1572880 | tf_op jit(solution)/shard_map/all_gather | solution.py:319
  68.0 44.7 %all-gather.7.cloned.1.call-done.v = bf16[3072,256]{1,0:T(8,128)(2,1)} async-done(((bf16[384,256]{1,0:T(8,128)(2,1)}), bf16[3072,256]{1,0:T(8,128)(2,1)}) %all-gather.7.cloned.1.call-update) | async-done | bytes 1572880 | tf_op jit(solution)/shard_map/all_gather | solution.py:320
  112.8 27.9 %attention.1 = (bf16[384,256]{1,0:T(8,128)(2,1)}, f32[384,128]{1,0:T(8,128)}) custom-call(bf16[384,256]{1,0:T(8,128)(2,1)} %get-tuple-element.8.q, bf16[3072,256]{1,0:T(8,128)(2,1)} %all-gather.5.cloned.1.call-done.k, bf16[3072,256]{1,0:T(8,128)(2,1)} %all-gather.7.cloned.1.call-done.v, bf16[8,2,384]{2,1,0:T(2,128)(2,1)} %all-gather.1.bias), custom_call_target="tpu_custom_call" | custom-call | tf_op jit(solution)/shard_map/attention/pallas_call | solution.py:337
  140.6 0.0 copy-start.1
  140.6 15.8 %mix.1 = bf16[96,2048]{1,0:T(8,128)(2,1)} custom-call(bf16[384,256]{1,0:T(8,128)(2,1)} %get-tuple-element.11.att, f32[384,256]{1,0:T(8,128)} %bitcast_add_fusion.conv, bf16[4,1,256]{2,1,0:T(2,128)(2,1)} %reshape.18.gain, bf16[1024,2048]{1,0:T(8,128)(2,1)} %wa.1, bf16[1024,2048]{1,0:T(8,128)(2,1)} %wc.1), custom_call_target="tpu_custom_call" | custom-call | tf_op jit(solution)/shard_map/mix/pallas_call | solution.py:355
  156.4 0.0 copy-done.1
  156.4 0.1 log_bitcast_fusion
  156.5 0.7 copy.31
  157.2 1.8 %copy.39 = bf16[96,2048]{1,0:T(8,128)(2,1)} copy(bf16[96,2048]{1,0:T(8,128)(2,1)} %mix.1) | data formatting | bytes 786432
  (1 shorter events, 0.0 us)
Async XLA Ops:
  7.2 21.9 %copy-start = (bf16[31,1024]{1,0:T(8,128)(2,1)S(1)}, bf16[31,1024]{1,0:T(8,128)(2,1)}, u32[]{:S(2)}) copy-start(bf16[31,1024]{1,0:T(8,128)(2,1)} %param.21) | copy-start | bytes 190468
  7.2 22.7 %copy-start.2 = (bf16[1024]{0:T(1024)(128)(2,1)S(1)}, bf16[1024]{0:T(1024)(128)(2,1)}, u32[]{:S(2)}) copy-start(bf16[1024]{0:T(1024)(128)(2,1)} %param.23) | copy-start | bytes 6148
  7.2 23.3 %copy-start.3 = (bf16[2,384]{1,0:T(2,128)(2,1)S(1)}, bf16[2,384]{1,0:T(2,128)(2,1)}, u32[]{:S(2)}) copy-start(bf16[2,384]{1,0:T(2,128)(2,1)} %param.18) | copy-start | bytes 4612
  7.2 60.8 %all-gather.5.cloned.1.call-start = ((), (), s32[]{:S(2)}) async-start(), calls=%async_computation | async-start | bytes 1769472 | tf_op jit(solution)/shard_map/all_gather | solution.py:319
  26.3 86.5 %all-gather.7.cloned.1.call-start = ((), (), s32[]{:S(2)}) async-start(), calls=%async_computation.1 | async-start | bytes 1769472 | tf_op jit(solution)/shard_map/all_gather | solution.py:320
  27.8 23.7 %collective-permute-start = (bf16[30,256]{1,0:T(8,128)(2,1)S(1)}, bf16[30,256]{1,0:T(8,128)(2,1)S(1)}, u32[]{:S(2)}, u32[]{:S(2)}) collective-permute-start(bf16[30,256]{1,0:T(8,128)(2,1)S(1)} %slice.6), channel_id=1, source_target_pairs={{0,4},{4,8},{8,12},{12,16},{16,20},{20,24},{24,28},{1,5},{5,9},{9,... | collective-permute-start | bytes 46088 | tf_op jit(solution)/shard_map/ppermute | solution.py:20
  140.6 15.8 %copy-start.1 = (f32[384,128]{1,0:T(8,128)S(1)}, f32[384,128]{1,0:T(8,128)}, u32[]{:S(2)}) copy-start(f32[384,128]{1,0:T(8,128)} %get-tuple-element.13) | copy-start | bytes 589828
Sparse Core Ops, SparseCore 0:
  26.4 41.5 all-gather.4
  70.2 42.5 all-gather.6

commit v2 on v1

--- a/solution.py
+++ b/solution.py
@@ -158,45 +158,119 @@
     later[...] = (row_ids > col_ids).astype(jnp.float32).astype(jnp.bfloat16)
 
 
-def attention_kernel(tile, q, k, v, bias, att, carried_out, later, total, carried):
+def place_of(index, n):
+    odd = index % 2
+    return (1 - odd) * (index // 2) + odd * (n - 1 - index // 2)
+
+
+def index_at(place, n):
+    back = place // (n // 2)
+    return (1 - back) * (2 * place) + back * (2 * (n - 1 - place) + 1)
+
+
+def attention_kernel(
+    n, tile, q, k, v, bias, att, carried_out, k_slots, v_slots, b_slots, later, outs, kept,
+    carried, send, recv
+):
     me = lax.axis_index("sp")
+    place = place_of(me, n)
     rows, width = q.shape
     heads = width // HEAD
+    half = n // 2
+    own = (k, v, bias)
+    slots = (k_slots, v_slots, b_slots)
+
+    def seat(distance):
+        return index_at((place + distance + n) % n, n)
+
+    sides = (1, -1)
+    greet([seat(1), seat(-1)], "sp")
+
+    def copy_of(side, turn, i, first):
+        owner = seat(-sides[side] * turn)
+        return pltpu.make_async_remote_copy(
+            src_ref=own[i] if first else slots[i].at[owner],
+            dst_ref=slots[i].at[owner],
+            send_sem=send.at[side, i, turn],
+            recv_sem=recv.at[side, i, turn],
+            device_id={"sp": seat(sides[side])},
+            device_id_type=MESH,
+        )
+
+    for side in range(2):
+        for i in range(3):
+            copy_of(side, 0, i, True).start()
     fill_later(later)
 
-    def block_step(block, masked):
-        begin = pl.multiple_of(block * rows, rows)
+    def process(block, refs, masked):
         for head in range(heads):
             cols = pl.ds(head * HEAD, HEAD)
-            keys = k[pl.ds(begin, rows), cols]
-            values = v[pl.ds(begin, rows), cols]
-            offsets = bias[block, pl.ds(head, 1), :].astype(jnp.float32)
+            keys, values = refs[0][:, cols], refs[1][:, cols]
+            offsets = refs[2][pl.ds(head, 1), :].astype(jnp.float32)
             for start in range(0, rows, tile):
                 part = pl.ds(start, tile)
-                out, kept = attention_tile(
+                out, total = attention_tile(
                     q[part, cols], keys, values, offsets, later[...], start, masked
                 )
-                if masked:
-                    total[part, cols] = out
-                    carried[head, part, :] = kept
-                else:
-                    before = carried[head, part, :]
-                    total[part, cols] = total[part, cols] + jnp.exp(before) * out
-                    carried[head, part, :] = before + kept
-
-    block_step(me, True)
-
-    def absorb(turn, state):
-        block_step(me - 1 - turn, False)
+                outs[block, part, cols] = out
+                kept[block, head, part, :] = total
+
+    def absorb(block):
+        @pl.when(block < me)
+        def _():
+            process(block, [slot.at[block] for slot in slots], False)
+
+    process(me, own, True)
+
+    def arrive(side, turn):
+        for i in range(3):
+            copy_of(side, turn, i, False).wait_recv()
+
+    def onward(side, turn):
+        for i in range(3):
+            copy_of(side, turn, i, False).start()
+
+    def step(turn, state):
+        arrive(0, turn)
+        onward(0, turn + 1)
+        arrive(1, turn)
+
+        @pl.when(turn < half - 2)
+        def _():
+            onward(1, turn + 1)
+
+        def each(side, inner):
+            absorb(seat((2 * side - 1) * (turn + 1)))
+            return inner
+
+        return lax.fori_loop(0, 2, each, state)
+
+    lax.fori_loop(0, half - 1, step, 0)
+    arrive(0, half - 1)
+    absorb(seat(-half))
+    for head in range(heads):
+        carried[head] = kept[me, head]
+
+    def combine(turn, state):
+        block = me - 1 - turn
+        for head in range(heads):
+            cols = pl.ds(head * HEAD, HEAD)
+            before = carried[head]
+            outs[me, :, cols] = outs[me, :, cols] + jnp.exp(before) * outs[block, :, cols]
+            carried[head] = before + kept[block, head]
         return state
 
-    lax.fori_loop(0, me, absorb, 0)
-    att[...] = total[...].astype(jnp.bfloat16)
+    lax.fori_loop(0, me, combine, 0)
+    att[...] = outs[me].astype(jnp.bfloat16)
     lanes = lax.broadcasted_iota(jnp.int32, carried_out.shape, 1)
     result = jnp.zeros(carried_out.shape, jnp.float32)
     for head in range(heads):
         result = jnp.where(lanes == head, carried[head], result)
     carried_out[...] = result
+    for side in range(2):
+        for turn in range(half - side):
+            for i in range(3):
+                copy_of(side, turn, i, turn == 0).wait_send()
 
 
 def mix_kernel(n, tile, att, conv, gain, wa, wc, out, att_slots, conv_slots, both, send, recv):
@@ -316,9 +390,6 @@
     )
     rim_width = conv_weight.shape[0] - 1
     rim_rows = from_behind(gated[tok_rows - rim_width :], "sp", 1)
-    every_key = lax.all_gather(key_rows, "sp", axis=0, tiled=True)
-    every_value = lax.all_gather(value_rows, "sp", axis=0, tiled=True)
-    every_bias = lax.all_gather(key_bias, "sp", axis=0, tiled=False)
     channel_start = tp_index * channels_here
     taps_here = lax.dynamic_slice_in_dim(conv_weight, channel_start, channels_here, 1)
     bias_here = lax.dynamic_slice_in_dim(conv_bias, channel_start, channels_here, 0).astype(f32)
@@ -335,7 +406,7 @@
     convolved = convolved + bias_here[None, :]
     tile = largest_tile(tok_rows, 128)
     attended, carried = pl.pallas_call(
-        functools.partial(attention_kernel, tile),
+        functools.partial(attention_kernel, sp_count, tile),
         out_shape=[
             jax.ShapeDtypeStruct((tok_rows, width), bf16),
             jax.ShapeDtypeStruct((tok_rows, 128), f32),
@@ -343,13 +414,21 @@
         in_specs=vmem_specs(4),
         out_specs=vmem_specs(2),
         scratch_shapes=[
+            pltpu.VMEM((sp_count, tok_rows, width), bf16),
+            pltpu.VMEM((sp_count, tok_rows, width), bf16),
+            pltpu.VMEM((sp_count, heads_here, tok_rows), bf16),
             pltpu.VMEM((tok_rows, tok_rows), bf16),
-            pltpu.VMEM((tok_rows, width), f32),
+            pltpu.VMEM((sp_count, tok_rows, width), f32),
+            pltpu.VMEM((sp_count, heads_here, tok_rows, 1), f32),
             pltpu.VMEM((heads_here, tok_rows, 1), f32),
+            pltpu.SemaphoreType.DMA((2, 3, sp_count // 2)),
+            pltpu.SemaphoreType.DMA((2, 3, sp_count // 2)),
         ],
-        compiler_params=pltpu.CompilerParams(vmem_limit_bytes=VMEM_LIMIT),
+        compiler_params=pltpu.CompilerParams(
+            collective_id=2, has_side_effects=True, vmem_limit_bytes=VMEM_LIMIT
+        ),
         name="attention",
-    )(query, every_key, every_value, every_bias)
+    )(query, key_rows, value_rows, key_bias)
     weight_log = jnp.log(-jnp.expm1(carried[:, :heads_here].T))
     mine = tok_rows // n
     mixed = pl.pallas_call(

time: 166 us -> 95.8 us (0.58)
  waiting for transfers between devices: 54.7 us -> 0.01 us
  blocking collectives: 21 us -> 0 us
  Pallas kernels: 61.4 us -> 78.8 us
  between operations: 14.1 us -> 0.71 us
    all_gather x2 -> x0, waiting for transfers between devices: 54 us -> none  [the longest x1 44.7 us: on_device(): every_value = lax.all_gather(value_rows, 'sp', axis=0, tiled=True)]
    all_gather x1 -> x0, blocking collectives: 21 us -> none  [on_device(): every_bias = lax.all_gather(key_bias, 'sp', axis=0, tiled=False)]
    pallas_call x1, Pallas kernels: 27.9 us -> 43.9 us  [on_device(): pl.pallas_call(functools.partial(attention_kernel, sp_count, tile), out_s...]
  transfers between devices with their start and end apart: 3 -> 1, of which waited for: 2 -> 0; matrix products, arithmetic and copies ran while one was open for 6% -> 3% of each run, Pallas kernels for 0% -> 46%
where the time goes in v2:
time: 95.8 us; the launch traced here: 95.1 us
  Pallas kernels  78.8 us (82%)
  matrix products  5.62 us (6%)
  local copies, waits for them, and re-layouts  5.13 us (5%)
  other arithmetic  3.53 us (4%)
  starting transfers between devices  1.28 us (1%)
    pallas_call x1, Pallas kernels, on_device(): pl.pallas_call(functools.partial(attention_kernel, sp_count, tile), out_s...  43.9 us
    pallas_call x1, Pallas kernels, on_device(): pl.pallas_call(functools.partial(project_kernel, n, chunks), out_shape=[j...  17.7 us
    pallas_call x1, Pallas kernels, on_device(): pl.pallas_call(functools.partial(mix_kernel, n, largest_tile(model_width,...  17.2 us
    conv_general_dilated x1, matrix products, on_device(): lax.conv_general_dilated(extended[None], taps_here[:, None, :], (1,), [(0...  5.62 us
    unnamed x6, local copies, waits for them, and re-layouts  2.47 us
  transfers between devices with their start and end apart: 1, of which 0 were waited for; matrix products, arithmetic and copies ran while one was open for 3% of the time, Pallas kernels for 46%

profile of v2, /device:TPU:29, one launch (start us, length us, event | category | flops | bytes accessed | tf_op | source)
XLA Modules:
  0.0 95.1 jit_solution(7826881346782075301)
XLA Ops:
  0.6 0.0 copy-start
  0.6 0.0 copy-start.1
  0.7 1.3 %reshape.13.gain = bf16[4,1,512]{2,1,0:T(2,128)(2,1)} reshape(bf16[2048]{0:T(1024)(128)(2,1)} %param.14) | data formatting | bytes 8192 | tf_op jit(solution)/shard_map/reshape | solution.py:384
  2.0 17.7 %project.1 = (bf16[384,256]{1,0:T(8,128)(2,1)}, bf16[384,256]{1,0:T(8,128)(2,1)}, bf16[384,256]{1,0:T(8,128)(2,1)}, bf16[384,256]{1,0:T(8,128)(2,1)}) custom-call(bf16[384,512]{1,0:T(8,128)(2,1)} %tok.1, bf16[4,1,512]{2,1,0:T(2,128)(2,1)} %reshape.13.gain, bf16[2048,256]{1,0:T(8,128)(2,1)} %wq.1, bf16[2048,256]{1,0:T(8,128)(2,1)} %wk.1, ...), custom_call_target="tpu_custom_call" | custom-call | tf_op jit(solution)/shard_map/project/pallas_call | solution.py:366
  19.7 0.7 slice.6
  20.4 1.3 %collective-permute-start = (bf16[30,256]{1,0:T(8,128)(2,1)S(1)}, bf16[30,256]{1,0:T(8,128)(2,1)S(1)}, u32[]{:S(2)}, u32[]{:S(2)}) collective-permute-start(bf16[30,256]{1,0:T(8,128)(2,1)S(1)} %slice.6), channel_id=1, source_target_pairs={{0,4},{4,8},{8,12},{12,16},{16,20},{20,24},{24,28},{1,5},{5,9},{9,... | collective-permute-start | bytes 46088 | tf_op jit(solution)/shard_map/ppermute | solution.py:20
  21.7 43.9 %attention.1 = (bf16[384,256]{1,0:T(8,128)(2,1)}, f32[384,128]{1,0:T(8,128)}) custom-call(bf16[384,256]{1,0:T(8,128)(2,1)} %get-tuple-element.8.q, bf16[384,256]{1,0:T(8,128)(2,1)} %get-tuple-element.9.k, bf16[384,256]{1,0:T(8,128)(2,1)} %get-tuple-element.10.v, bf16[2,384]{1,0:T(2,128)(2,1)} %bias.1), custom_call_target="tpu_custom_call" | custom-call | tf_op jit(solution)/shard_map/attention/pallas_call | solution.py:408
  65.6 1.0 %log_bitcast_fusion = f32[2,384]{0,1:T(8,128)S(1)} fusion(f32[384,128]{1,0:T(8,128)} %get-tuple-element.13), kind=kLoop, calls=%fused_computation.4 | loop fusion | flops 768 | bytes 6144 | tf_op jit(solution)/shard_map/log | solution.py:432
  66.6 0.0 copy-done
  66.6 0.8 dynamic-slice_convert_fusion
  67.4 0.0 copy-done.1
  67.4 0.6 reshape.14.gain
  68.0 0.7 copy.26
  68.7 0.0 collective-permute-done
  68.7 1.0 %maximum_bitcast_fusion = bf16[1,414,256]{2,1,0:T(8,128)(2,1)S(1)} fusion(bf16[384,256]{1,0:T(8,128)(2,1)} %get-tuple-element.12, bf16[30,256]{1,0:T(8,128)(2,1)S(1)} %collective-permute-done), kind=kLoop, calls=%fused_computation.3 | loop fusion | flops 423936 | bytes 423936 | tf_op jit(solution)/shard_map/broadcast_in_dim | solution.py:398
  69.7 5.6 %fusion = f32[1,384,256]{2,0,1:T(1,128)S(1)} fusion(bf16[1,414,256]{2,1,0:T(8,128)(2,1)S(1)} %maximum_bitcast_fusion, bf16[31,1,256]{2,0,1:T(8,128)(2,1)S(1)} %dynamic-slice_bitcast_fusion), kind=kOutput, calls=%fused_computation | convolution fusion | flops 6094848 | bytes 621056 | tf_op jit(solution)/shard_map/conv_general_dilated | solution.py:397
  75.3 0.8 bitcast_add_fusion.conv
  76.1 17.2 %mix.1 = bf16[96,2048]{1,0:T(8,128)(2,1)} custom-call(bf16[384,256]{1,0:T(8,128)(2,1)} %get-tuple-element.11.att, f32[384,256]{1,0:T(8,128)} %bitcast_add_fusion.conv, bf16[4,1,256]{2,1,0:T(2,128)(2,1)} %reshape.14.gain, bf16[1024,2048]{1,0:T(8,128)(2,1)} %wa.1, bf16[1024,2048]{1,0:T(8,128)(2,1)} %wc.1), custom_call_target="tpu_custom_call" | custom-call | tf_op jit(solution)/shard_map/mix/pallas_call | solution.py:434
  93.3 1.8 %copy.34 = bf16[96,2048]{1,0:T(8,128)(2,1)} copy(bf16[96,2048]{1,0:T(8,128)(2,1)} %mix.1) | data formatting | bytes 786432
  (1 shorter events, 0.0 us)
Async XLA Ops:
  0.6 66.0 %copy-start = (bf16[31,1024]{1,0:T(8,128)(2,1)S(1)}, bf16[31,1024]{1,0:T(8,128)(2,1)}, u32[]{:S(2)}) copy-start(bf16[31,1024]{1,0:T(8,128)(2,1)} %param.21) | copy-start | bytes 190468
  0.6 66.8 %copy-start.1 = (bf16[1024]{0:T(1024)(128)(2,1)S(1)}, bf16[1024]{0:T(1024)(128)(2,1)}, u32[]{:S(2)}) copy-start(bf16[1024]{0:T(1024)(128)(2,1)} %param.23) | copy-start | bytes 6148
  20.4 48.3 %collective-permute-start = (bf16[30,256]{1,0:T(8,128)(2,1)S(1)}, bf16[30,256]{1,0:T(8,128)(2,1)S(1)}, u32[]{:S(2)}, u32[]{:S(2)}) collective-permute-start(bf16[30,256]{1,0:T(8,128)(2,1)S(1)} %slice.6), channel_id=1, source_target_pairs={{0,4},{4,8},{8,12},{12,16},{16,20},{20,24},{24,28},{1,5},{5,9},{9,... | collective-permute-start | bytes 46088 | tf_op jit(solution)/shard_map/ppermute | solution.py:20
